TPU v7x, 512 devices: a whole 4x8x8 slice. The times are simulated.
512 devices in a mesh: ep: 32 (over z, x), tp: 16 (over y, core).
Axes of the slice: x: 4, y: 8, z: 8, core: 2. Of those that a mesh axis runs over, the one named last changes fastest.
Arguments:
- tokens: bfloat16 [256, 2048], P('ep', 'tp'), may hold values from -10 to 10, as said below
- norm_gain: float32 [2048], P('tp'), may hold values from 0.5 to 1.5
- norm_bias: float32 [2048], P('tp'), may hold values from -0.3 to 0.3
- group_pick: int32 [256, 1], P('ep'), may hold values from 0 to 7; in each aligned block of 8 rows (0 to 7, 8 to 15, ...) at most 2 rows name the same one
- member_pick: int32 [256, 4], P('ep'), may hold values from 0 to 7, all different within a row
- picked_probs: float32 [256, 4], P('ep'), may hold values from 0.05 to 1
- gate_weight: bfloat16 [64, 2048, 1024], P('ep', 'tp'), may hold values from -0.125 to 0.125
- up_weight: bfloat16 [64, 2048, 1024], P('ep', 'tp'), may hold values from -0.125 to 0.125
- down_weight: bfloat16 [64, 1024, 2048], P('ep', None, 'tp'), may hold values from -0.375 to 0.375
Outputs:
- mixed: bfloat16 [256, 2048], P('ep', 'tp')
Inputs may be any that keep to these rules, and one draw needn't show every extreme that they name: `group_pick`: each entry is a group number from 0 to 7; within each aligned block of 8 tokens no group is named by more than 2 tokens, a bound that some block reaches. `member_pick`: each token's 4 entries are different member numbers from 0 to 7. `tokens`: each token is its own offset between -2 and 2 plus its own scale between 0.25 and 2 times entries of at most 4 in size.
All inputs are finite; a program needn't handle non-finite values.
Results may differ from a plain program's by a relative error of at most 0.01.
Values may be sent and summed in bfloat16 or wider, within the bound.
A program may use at most 64 MiB of HBM per device.

v0:
```python
import functools

import jax
import jax.numpy as jnp
from jax import lax
from jax.experimental import pallas as pl
from jax.experimental.pallas import tpu as pltpu
from jax.sharding import PartitionSpec as P

EPG = 8
CORES = 2
LANES = 128
norm_epsilon = 1e-05
MESH = pl.DeviceIdType.MESH
F32 = jnp.float32
BF16 = jnp.bfloat16


def iota(shape, dim):
    return lax.broadcasted_iota(jnp.int32, shape, dim)


def kernel(
    E, T, G, cap,
    tokens_h, gain_h, bias_h, group_h, member_h, probs_h, gate_h, up_h, down_h,
    out_ref,
    tokens_v, gain_v, bias_v, group_v, member_v, probs_v, gate_v, up_v, down_v,
    info_out, info_in, info_all, rows_out, rows_in, rows_all,
    core_out, core_in, y_out, y_in, held, hid_own, hid_other, back_out, back_in,
    local_sem, weight_sem,
    info_s, info_r, rows_s, rows_r,
    core_s, core_r, y_s, y_r, hid_s, hid_r, back_s, back_r,
):
    n, width = tokens_h.shape
    LE = gate_h.shape[0]
    FF = gate_h.shape[2]
    half = FF // CORES
    NY = T // CORES
    S = G * cap
    R = E * cap
    group_devices = EPG // LE
    me = lax.axis_index("ep")
    mt = lax.axis_index("tp")
    core = lax.rem(mt, CORES)
    my = lax.div(mt, CORES)

    def ep_at(d):
        return lax.rem(me + d, E)

    def tp_at(d):
        return lax.rem(mt + d, T)

    def remote(src, dst, ssem, rsem, ep, tp):
        return pltpu.make_async_remote_copy(
            src_ref=src, dst_ref=dst, send_sem=ssem, recv_sem=rsem,
            device_id=(ep, tp), device_id_type=MESH,
        )

    barrier = pltpu.get_barrier_semaphore()
    others = [(d, t) for t in range(T) for d in range(E) if d or t]
    eps = [ep_at(d) for d in range(E)]
    tps = [tp_at(d) for d in range(T)]
    for d, t in others:
        pl.semaphore_signal(barrier, inc=1, device_id=(eps[d], tps[t]), device_id_type=MESH)

    small = [
        pltpu.make_async_copy(h, v, local_sem.at[i])
        for i, (h, v) in enumerate(
            ((group_h, group_v), (member_h, member_v), (probs_h, probs_v),
             (tokens_h, tokens_v), (gain_h, gain_v), (bias_h, bias_v))
        )
    ]
    for c in small:
        c.start()
    weights = [
        [pltpu.make_async_copy(h.at[j], v.at[j], weight_sem.at[w, j]) for j in range(LE)]
        for w, (h, v) in enumerate(((gate_h, gate_v), (up_h, up_v), (down_h, down_v)))
    ]
    for w in range(2):
        for j in range(LE):
            weights[w][j].start()
    for j in range(LE):
        weights[2][j].start()
    for c in small:
        c.wait()

    lane = iota((n, n), 1)
    sub = iota((n, n), 0)

    def column(row):
        wide = jnp.broadcast_to(row, (n, n))
        return jnp.sum(jnp.where(lane == sub, wide, 0.0), axis=1, keepdims=True)

    group_row = group_v[...].astype(F32)
    group_col = column(group_row)
    same = jnp.where(group_col == group_row, 1.0, 0.0)
    slot_row = jnp.sum(jnp.where(sub < lane, same, 0.0), axis=0, keepdims=True)
    slot_col = jnp.sum(jnp.where(lane < sub, same, 0.0), axis=1, keepdims=True)
    key_row = group_row * cap + slot_row
    key_col = group_col * cap + slot_col
    place = jnp.where(key_row == iota((S, n), 0).astype(F32), 1.0, 0.0)

    def pack(v):
        total = place[:, 0:1] * v[0:1, :]
        for t in range(1, n):
            total += place[:, t : t + 1] * v[t : t + 1, :]
        return total

    probs = probs_v[...]
    member = member_v[...].astype(F32)
    shares = probs / jnp.sum(probs, axis=0, keepdims=True)
    values = tokens_v[...].astype(F32)
    center_here = jnp.sum(values, axis=1, keepdims=True) / width
    away = values - center_here
    square_here = jnp.sum(away * away, axis=1, keepdims=True)
    spot = iota((n, LANES), 1).astype(F32)
    info = jnp.where(spot == slot_col, center_here, 0.0)
    info += jnp.where(spot == slot_col + cap, square_here, 0.0)
    for k in range(probs.shape[0]):
        hit = spot == (column(member[k : k + 1, :]) + 2) * cap + slot_col
        info += jnp.where(hit, column(shares[k : k + 1, :]), 0.0)
    packed = pack(values)
    for g in range(G):
        info_out[g] = jnp.sum(jnp.where(group_col == g, info, 0.0), axis=0, keepdims=True)
        rows_out[g] = packed[g * cap : (g + 1) * cap, :].astype(BF16)

    pl.semaphore_wait(barrier, len(others))

    groups = [lax.div(p, group_devices) for p in eps]
    sent = []
    for d in range(1, E):
        c = remote(
            rows_out.at[groups[d]], rows_in.at[d], rows_s.at[d], rows_r.at[d], eps[d], mt,
        )
        c.start()
        sent.append(c)
    told = []
    for d, t in others:
        c = remote(
            info_out.at[groups[d]], info_in.at[d, t], info_s.at[d, t], info_r.at[d, t],
            eps[d], tps[t],
        )
        c.start()
        told.append(c)
    rows_in[0] = rows_out[groups[0]]
    info_in[0, 0] = info_out[groups[0]]
    gain = gain_v[...]
    bias = bias_v[...]
    for w in range(2):
        for j in range(LE):
            weights[w][j].wait()
    for c in sent:
        c.wait_recv()
    for d in range(E):
        rows_all[d * cap : (d + 1) * cap, :] = rows_in[d].astype(F32)
    for c in told:
        c.wait_recv()
    for t in range(T):
        for d in range(E):
            info_all[t, d * cap : (d + 1) * cap, :] = jnp.broadcast_to(info_in[d, t], (cap, LANES))
    rlane = iota((R, LANES), 1)
    rslot = lax.rem(iota((R, LANES), 0), cap)

    def fact(t, kind):
        return jnp.sum(
            jnp.where(rlane == kind * cap + rslot, info_all[t], 0.0), axis=1, keepdims=True
        )

    centers = [fact(t, 0) for t in range(T)]
    center = sum(centers) / T
    square = sum(fact(t, 1) + width * (c - center) * (c - center) for t, c in enumerate(centers))
    spread = square / (width * T)
    normed = (rows_all[...] - center) * lax.rsqrt(spread + norm_epsilon) * gain + bias
    rows = normed.astype(BF16)

    mine = pl.ds(pl.multiple_of(core * half, half), half)
    theirs = pl.ds(pl.multiple_of((1 - core) * half, half), half)
    partner = my * CORES + (1 - core)
    to_core = []
    for j in range(LE):
        for w, v in enumerate((gate_v, up_v)):
            core_out[j, w] = jnp.dot(rows, v[j, :, theirs], preferred_element_type=F32).astype(BF16)
        c = remote(core_out.at[j], core_in.at[j], core_s.at[j], core_r.at[j], me, partner)
        c.start()
        to_core.append(c)
    to_y = []
    for j in range(LE):
        for w, v in enumerate((gate_v, up_v)):
            held[j, w] = jnp.dot(rows, v[j, :, mine], preferred_element_type=F32)
        to_core[j].wait_recv()
        for w in range(2):
            total = held[j, w] + core_in[j, w].astype(F32)
            held[j, w] = total
            y_out[j, w] = total.astype(BF16)
        copies = []
        for d in range(1, NY):
            c = remote(
                y_out.at[j], y_in.at[j, d - 1], y_s.at[j, d - 1], y_r.at[j, d - 1],
                me, lax.rem(my + d, NY) * CORES + core,
            )
            c.start()
            copies.append(c)
        to_y.append(copies)
    for j in range(LE):
        weights[2][j].wait()
    to_hid = []
    partial = []
    for j in range(LE):
        gate = held[j, 0]
        up = held[j, 1]
        for d in range(1, NY):
            to_y[j][d - 1].wait_recv()
            gate += y_in[j, d - 1, 0].astype(F32)
            up += y_in[j, d - 1, 1].astype(F32)
        hidden = (gate / (1.0 + jnp.exp(-gate)) * up).astype(BF16)
        hid_own[j] = hidden
        c = remote(hid_own.at[j], hid_other.at[j], hid_s.at[j], hid_r.at[j], me, partner)
        c.start()
        to_hid.append(c)
        partial.append(jnp.dot(hidden, down_v[j, mine, :], preferred_element_type=F32))
    total = jnp.zeros((R, width), F32)
    for j in range(LE):
        to_hid[j].wait_recv()
        expert = partial[j] + jnp.dot(hid_other[j], down_v[j, theirs, :], preferred_element_type=F32)
        which = lax.rem(me * LE + j, EPG)
        weight = fact(0, which + 2)
        total += weight * expert.astype(BF16).astype(F32)

    back = []
    for d in range(1, E):
        back_out[d] = total[d * cap : (d + 1) * cap, :].astype(BF16)
        c = remote(
            back_out.at[d], back_in.at[me], back_s.at[d - 1], back_r.at[d - 1],
            lax.rem(me - d + E, E), mt,
        )
        c.start()
        back.append(c)
    back_in[me] = total[0:cap, :].astype(BF16)
    for c in told:
        c.wait_send()
    for c in sent:
        c.wait_send()
    for j in range(LE):
        to_core[j].wait_send()
        to_hid[j].wait_send()
        for c in to_y[j]:
            c.wait_send()
    for c in back:
        c.wait()
    finder = jnp.where(key_col == iota((n, LANES), 1).astype(F32), 1.0, 0.0)
    mixed = jnp.zeros((n, width), F32)
    for g in range(G):
        part = back_in[g * group_devices].astype(F32)
        for p in range(1, group_devices):
            part += back_in[g * group_devices + p].astype(F32)
        for s in range(cap):
            at = g * cap + s
            mixed += finder[:, at : at + 1] * part[s : s + 1, :]
    out_ref[...] = mixed


def per_device(E, T, tokens, norm_gain, norm_bias, group_pick, member_pick, picked_probs,
               gate_weight, up_weight, down_weight):
    n, width = tokens.shape
    LE, _, FF = gate_weight.shape
    half = FF // CORES
    NY = T // CORES
    G = LE * E // EPG
    cap = max(n // 4, (n + G - 1) // G)
    S = G * cap
    R = E * cap
    k = picked_probs.shape[1]
    dma = pltpu.SemaphoreType.DMA
    V = pltpu.VMEM
    scratch = [
        V((n, width), BF16), V((1, width), F32), V((1, width), F32),
        V((1, n), jnp.int32), V((k, n), jnp.int32), V((k, n), F32),
        V((LE, width, FF), BF16), V((LE, width, FF), BF16), V((LE, FF, width), BF16),
        V((G, 1, LANES), F32), V((E, T, 1, LANES), F32), V((T, R, LANES), F32),
        V((G, cap, width), BF16), V((E, cap, width), BF16), V((R, width), F32),
        V((LE, 2, R, half), BF16), V((LE, 2, R, half), BF16),
        V((LE, 2, R, half), BF16), V((LE, NY - 1, 2, R, half), BF16),
        V((LE, 2, R, half), F32),
        V((LE, R, half), BF16), V((LE, R, half), BF16),
        V((E, cap, width), BF16), V((E, cap, width), BF16),
        dma((6,)), dma((3, LE)),
        dma((E, T)), dma((E, T)), dma((E,)), dma((E,)),
        dma((LE,)), dma((LE,)), dma((LE, NY - 1)), dma((LE, NY - 1)), dma((LE,)), dma((LE,)),
        dma((E - 1,)), dma((E - 1,)),
    ]
    anywhere = pl.BlockSpec(memory_space=pl.ANY)
    combined = pl.pallas_call(
        functools.partial(kernel, E, T, G, cap),
        out_shape=jax.ShapeDtypeStruct((n, width), F32),
        in_specs=[anywhere] * 9,
        out_specs=pl.BlockSpec(memory_space=pltpu.VMEM),
        scratch_shapes=scratch,
        compiler_params=pltpu.CompilerParams(collective_id=0, has_side_effects=True),
        name="moe_step",
    )(tokens, norm_gain.reshape(1, width), norm_bias.reshape(1, width), group_pick.T, member_pick.T,
      picked_probs.T, gate_weight, up_weight, down_weight)
    return combined.astype(BF16)


def solution(mesh):
    placed = (
        P("ep", "tp"), P("tp"), P("tp"), P("ep", None), P("ep", None), P("ep", None),
        P("ep", "tp", None), P("ep", "tp", None), P("ep", None, "tp"),
    )
    body = functools.partial(per_device, mesh.shape["ep"], mesh.shape["tp"])
    return jax.shard_map(body, mesh=mesh, in_specs=placed, out_specs=P("ep", "tp"), check_vma=False)
```

profile of v0, /device:TPU:1, one launch (start us, length us, event | category | flops | bytes accessed | tf_op | source)
XLA Modules:
  0.0 114.6 jit_solution(14485381310453666825)
XLA Ops:
  0.0 113.3 %moe_step.1 = f32[8,128]{1,0:T(8,128)} custom-call(bf16[8,128]{1,0:T(8,128)(2,1)} %tokens_h.1, f32[1,128]{1,0:T(1,128)} %bitcast.7, f32[1,128]{1,0:T(1,128)} %bitcast.8, s32[1,8]{1,0:T(1,128)} %bitcast.9, s32[4,8]{1,0:T(4,128)} %bitcast.5, f32[4,8]{1,0:T(4,128)} %bitcast.6, bf16[2,128,1024]{2,1,0:T(8,128)(2,1)} %gate_h.1, bf16[2,128,1024]{2,1,0:T(8,128)(2,1)} %up_h.1, ...), custom_call_target="tpu_custom_call" | custom-call | tf_op jit(solution)/shard_map/moe_step/pallas_call | solution.py:292
  113.4 1.3 %convert_element_type.3 = bf16[8,128]{1,0:T(8,128)(2,1)} convert(f32[8,128]{1,0:T(8,128)} %moe_step.1) | non-fusion elementwise | flops 1024 | bytes 6144 | tf_op jit(solution)/shard_map/convert_element_type | solution.py:302
where the time goes:
time: 115 us
  Pallas kernels  113 us (98%)
  other arithmetic  1.26 us (1%)
    pallas_call x1, Pallas kernels, per_device(): pl.pallas_call(functools.partial(kernel, E, T, G, cap), out_shape=jax.Sha...  113 us

commit v1 on v0

v1 whole, which is shorter than its diff:
```python
import functools

import jax
import jax.numpy as jnp
from jax import lax
from jax.experimental import pallas as pl
from jax.experimental.pallas import tpu as pltpu
from jax.sharding import PartitionSpec as P

EPG = 8
CORES = 2
LANES = 128
ROW_CHIPS = 4
norm_epsilon = 1e-05
MESH = pl.DeviceIdType.MESH
F32 = jnp.float32
BF16 = jnp.bfloat16


def iota(shape, dim):
    return lax.broadcasted_iota(jnp.int32, shape, dim)


def around(d, size):
    return min(d, size - d)


def kernel(
    E, T, G, cap,
    tokens_h, gain_h, bias_h, group_h, member_h, probs_h, gate_h, up_h, down_h,
    out_ref,
    tokens_v, gain_v, bias_v, group_v, member_v, probs_v, gate_v, up_v, down_v,
    stats_out, stats_in, rows_out, rows_in, rows_all, info_all,
    core_out, core_in, y_out, y_in, hid_own, hid_other, back_out, back_in,
    local_sem, weight_sem,
    stats_s, stats_r, rows_s, rows_r,
    core_s, core_r, y_s, y_r, hid_s, hid_r, pass_s, pass_r, back_s, back_r,
):
    n, width = tokens_h.shape
    LE = gate_h.shape[0]
    FF = gate_h.shape[2]
    half = FF // CORES
    quarters = half // LANES
    NY = T // CORES
    R = E * cap
    rows_each = cap + 2
    group_devices = EPG // LE
    X = ROW_CHIPS
    Z = E // X
    me = lax.axis_index("ep")
    mt = lax.axis_index("tp")
    core = lax.rem(mt, CORES)
    my = lax.div(mt, CORES)
    mz = lax.div(me, X)
    mx = lax.rem(me, X)
    partner = my * CORES + (1 - core)

    def peer(d):
        dz, dx = divmod(d, X)
        return lax.rem(mz + dz, Z) * X + lax.rem(mx + dx, X)

    def source(d):
        dz, dx = divmod(d, X)
        return lax.rem(mz + Z - dz, Z) * X + lax.rem(mx + X - dx, X)

    def remote(src, dst, ssem, rsem, ep, tp):
        return pltpu.make_async_remote_copy(
            src_ref=src, dst_ref=dst, send_sem=ssem, recv_sem=rsem,
            device_id=(ep, tp), device_id_type=MESH,
        )

    ep_order = sorted(range(1, E), key=lambda d: -(around(d // X, Z) + around(d % X, X)))
    y_order = sorted(range(1, NY), key=lambda o: -around(o, NY))
    tp_order = sorted(range(1, T), key=lambda t: -around(t // CORES, NY))

    def tp_at(t):
        return lax.rem(my + t // CORES, NY) * CORES + lax.rem(core + t % CORES, CORES)

    def y_at(o):
        return lax.rem(my + o, NY)

    eps = {d: peer(d) for d in ep_order}
    tps = {t: tp_at(t) for t in tp_order}

    barrier = pltpu.get_barrier_semaphore()
    for d in ep_order:
        pl.semaphore_signal(barrier, inc=1, device_id=(eps[d], mt), device_id_type=MESH)
    for t in tp_order:
        pl.semaphore_signal(barrier, inc=1, device_id=(me, tps[t]), device_id_type=MESH)

    small = [
        pltpu.make_async_copy(h, v, local_sem.at[i])
        for i, (h, v) in enumerate(
            ((tokens_h, tokens_v), (group_h, group_v), (member_h, member_v), (probs_h, probs_v),
             (gain_h, gain_v), (bias_h, bias_v))
        )
    ]
    for c in small:
        c.start()
    weights = [
        [pltpu.make_async_copy(h.at[j], v.at[j], weight_sem.at[w, j]) for j in range(LE)]
        for w, (h, v) in enumerate(((gate_h, gate_v), (up_h, up_v), (down_h, down_v)))
    ]
    for w in range(3):
        for j in range(LE):
            weights[w][j].start()
    for c in small:
        c.wait()

    lane = iota((n, n), 1)
    sub = iota((n, n), 0)
    spot = iota((n, LANES), 1)
    spot_sub = iota((n, LANES), 0)

    values = tokens_v[...].astype(F32)
    center_here = jnp.sum(values, axis=1, keepdims=True) / width
    away = values - center_here
    square_here = jnp.sum(away * away, axis=1, keepdims=True)
    stats = jnp.where(spot == spot_sub, center_here, 0.0)
    stats += jnp.where(spot == spot_sub + n, square_here, 0.0)
    stats_row = jnp.sum(stats, axis=0, keepdims=True)
    stats_out[...] = stats_row

    def column(row):
        wide = jnp.broadcast_to(row, (n, n))
        return jnp.sum(jnp.where(lane == sub, wide, 0.0), axis=1, keepdims=True)

    group_row = group_v[...].astype(F32)
    group_col = column(group_row)
    same = jnp.where(group_col == group_row, 1.0, 0.0)
    slot_row = jnp.sum(jnp.where(sub < lane, same, 0.0), axis=0, keepdims=True)
    slot_col = jnp.sum(jnp.where(lane < sub, same, 0.0), axis=1, keepdims=True)
    key_col = group_col * cap + slot_col

    probs = probs_v[...]
    member = member_v[...].astype(F32)
    shares = probs / jnp.sum(probs, axis=0, keepdims=True)
    spot_f = spot.astype(F32)
    info = jnp.zeros((n, LANES), F32)
    for k in range(probs.shape[0]):
        hit = spot_f == column(member[k : k + 1, :]) * cap + slot_col
        info += jnp.where(hit, column(shares[k : k + 1, :]), 0.0)
    high = info.astype(BF16).astype(F32)
    low = info - high

    packed_row = iota((G * rows_each, n), 0).astype(F32)
    place = jnp.where(packed_row == group_row * rows_each + slot_row, 1.0, 0.0)
    place_high = jnp.where(packed_row == group_row * rows_each + cap, 1.0, 0.0)
    place_low = jnp.where(packed_row == group_row * rows_each + (cap + 1), 1.0, 0.0)
    base = jnp.zeros((G * rows_each, LANES), F32)
    for t in range(n):
        base += place_high[:, t : t + 1] * high[t : t + 1, :]
        base += place_low[:, t : t + 1] * low[t : t + 1, :]
    gain = gain_v[...]
    bias = bias_v[...]

    pl.semaphore_wait(barrier, E + T - 2)

    told = []
    for t in tp_order:
        c = remote(stats_out, stats_in.at[t], stats_s.at[t], stats_r.at[t], me, tps[t])
        c.start()
        told.append(c)
    for c in told:
        c.wait_recv()
    heard = [stats_row] + [stats_in[t] for t in range(1, T)]
    total = heard[0]
    for h in heard[1:]:
        total += h
    middle = total / T
    moved = jnp.zeros((1, LANES), F32)
    for h in heard:
        moved += (h - middle) * (h - middle)
    middle_wide = jnp.broadcast_to(middle, (n, LANES))
    total_wide = jnp.broadcast_to(total, (n, LANES))
    moved_wide = jnp.broadcast_to(moved, (n, LANES))
    center = jnp.sum(jnp.where(spot == spot_sub, middle_wide, 0.0), axis=1, keepdims=True)
    square = jnp.sum(
        jnp.where(spot == spot_sub + n, total_wide, 0.0)
        + jnp.where(spot == spot_sub, width * moved_wide, 0.0),
        axis=1, keepdims=True,
    )
    spread = square / (width * T)
    normed = (values - center) * lax.rsqrt(spread + norm_epsilon) * gain + bias
    packed = base
    for t in range(n):
        packed += place[:, t : t + 1] * normed[t : t + 1, :]
    for g in range(G):
        rows_out[g] = packed[g * rows_each : (g + 1) * rows_each, :].astype(BF16)

    sent = []
    for d in ep_order:
        c = remote(
            rows_out.at[lax.div(eps[d], group_devices)], rows_in.at[d],
            rows_s.at[d], rows_r.at[d], eps[d], mt,
        )
        c.start()
        sent.append(c)
    rows_in[0] = rows_out[lax.div(me, group_devices)]
    for w in range(2):
        for j in range(LE):
            weights[w][j].wait()
    for c in sent:
        c.wait_recv()
    for d in range(E):
        rows_all[d * cap : (d + 1) * cap, :] = rows_in[d, 0:cap, :].astype(F32)
    rows = rows_all[...].astype(BF16)

    def product(v, y, c):
        j = lax.div(y, quarters)
        at = c * half + lax.rem(y, quarters) * LANES
        block = v[j, :, pl.ds(pl.multiple_of(at, LANES), LANES)]
        return jnp.dot(rows, block, preferred_element_type=F32)

    to_core = {}
    for o in y_order + [0]:
        for w, v in enumerate((gate_v, up_v)):
            core_out[o, w] = product(v, y_at(o), 1 - core).astype(BF16)
        c = remote(core_out.at[o], core_in.at[o], core_s.at[o], core_r.at[o], me, partner)
        c.start()
        to_core[o] = c
    to_y = {}
    for o in y_order:
        mine = [product(v, y_at(o), core) for v in (gate_v, up_v)]
        to_core[o].wait_recv()
        for w in range(2):
            y_out[o, w] = (mine[w] + core_in[o, w].astype(F32)).astype(BF16)
        c = remote(
            y_out.at[o], y_in.at[o], y_s.at[o], y_r.at[o], me, y_at(o) * CORES + core,
        )
        c.start()
        to_y[o] = c
    mine = [product(v, my, core) for v in (gate_v, up_v)]
    to_core[0].wait_recv()
    gate = mine[0] + core_in[0, 0].astype(F32)
    up = mine[1] + core_in[0, 1].astype(F32)

    for d in range(E):
        block = rows_in[d].astype(F32)
        share_row = block[cap : cap + 1, :] + block[cap + 1 : cap + 2, :]
        info_all[d * cap : (d + 1) * cap, :] = jnp.broadcast_to(share_row, (cap, LANES))
    rlane = iota((R, LANES), 1)
    rslot = lax.rem(iota((R, LANES), 0), cap)
    info_rows = info_all[...]
    share_of = []
    for j in range(LE):
        which = lax.rem(me * LE + j, EPG)
        share_of.append(
            jnp.sum(jnp.where(rlane == which * cap + rslot, info_rows, 0.0), axis=1, keepdims=True)
        )
    finder = jnp.where(key_col == spot_f, 1.0, 0.0)

    for o in reversed(y_order):
        to_y[o].wait_recv()
        gate += y_in[o, 0].astype(F32)
        up += y_in[o, 1].astype(F32)
    hidden = (gate / (1.0 + jnp.exp(-gate)) * up).astype(BF16)
    hid_own[my] = hidden
    to_hid = {}
    for o in y_order:
        c = remote(
            hid_own.at[my], hid_own.at[my], hid_s.at[o], hid_r.at[o], me, y_at(o) * CORES + core,
        )
        c.start()
        to_hid[o] = c
    passed = []

    def forward(o):
        at = lax.rem(my + NY - o, NY)
        c = remote(hid_own.at[at], hid_other.at[at], pass_s.at[o], pass_r.at[o], me, partner)
        c.start()
        passed.append(c)

    forward(0)
    for o in reversed(y_order):
        to_hid[o].wait_recv()
        forward(o)
    for j in range(LE):
        weights[2][j].wait()

    def down(j, held, c):
        joined = jnp.concatenate([held[j * quarters + q] for q in range(quarters)], axis=1)
        part = down_v[j, pl.ds(pl.multiple_of(c * half, half), half), :]
        return jnp.dot(joined, part, preferred_element_type=F32)

    partial = [down(j, hid_own, core) for j in range(LE)]
    for c in passed:
        c.wait_recv()
    total = jnp.zeros((R, width), F32)
    for j in range(LE):
        expert = partial[j] + down(j, hid_other, 1 - core)
        total += share_of[j] * expert.astype(BF16).astype(F32)
    for d in range(E):
        back_out[d] = total[d * cap : (d + 1) * cap, :].astype(BF16)
    back = []
    for d in ep_order:
        c = remote(
            back_out.at[d], back_in.at[me], back_s.at[d], back_r.at[d], source(d), mt,
        )
        c.start()
        back.append(c)
    back_in[me] = back_out[0]
    for c in told + sent + list(to_core.values()) + list(to_y.values()):
        c.wait_send()
    for c in list(to_hid.values()) + passed:
        c.wait_send()
    for c in back:
        c.wait_recv()
    mixed = jnp.zeros((n, width), F32)
    for g in range(G):
        part = back_in[g * group_devices].astype(F32)
        for p in range(1, group_devices):
            part += back_in[g * group_devices + p].astype(F32)
        for s in range(cap):
            at = g * cap + s
            mixed += finder[:, at : at + 1] * part[s : s + 1, :]
    out_ref[...] = mixed
    for c in back:
        c.wait_send()


def per_device(E, T, tokens, norm_gain, norm_bias, group_pick, member_pick, picked_probs,
               gate_weight, up_weight, down_weight):
    n, width = tokens.shape
    LE, _, FF = gate_weight.shape
    NY = T // CORES
    G = LE * E // EPG
    cap = max(n // 4, (n + G - 1) // G)
    R = E * cap
    k = picked_probs.shape[1]
    dma = pltpu.SemaphoreType.DMA
    V = pltpu.VMEM
    scratch = [
        V((n, width), BF16), V((1, width), F32), V((1, width), F32),
        V((1, n), jnp.int32), V((k, n), jnp.int32), V((k, n), F32),
        V((LE, width, FF), BF16), V((LE, width, FF), BF16), V((LE, FF, width), BF16),
        V((1, LANES), F32), V((T, 1, LANES), F32),
        V((G, cap + 2, width), BF16), V((E, cap + 2, width), BF16), V((R, width), F32), V((R, LANES), F32),
        V((NY, 2, R, LANES), BF16), V((NY, 2, R, LANES), BF16),
        V((NY, 2, R, LANES), BF16), V((NY, 2, R, LANES), BF16),
        V((NY, R, LANES), BF16), V((NY, R, LANES), BF16),
        V((E, cap, width), BF16), V((E, cap, width), BF16),
        dma((6,)), dma((3, LE)),
        dma((T,)), dma((T,)), dma((E,)), dma((E,)),
        dma((NY,)), dma((NY,)), dma((NY,)), dma((NY,)), dma((NY,)), dma((NY,)), dma((NY,)), dma((NY,)),
        dma((E,)), dma((E,)),
    ]
    anywhere = pl.BlockSpec(memory_space=pl.ANY)
    combined = pl.pallas_call(
        functools.partial(kernel, E, T, G, cap),
        out_shape=jax.ShapeDtypeStruct((n, width), F32),
        in_specs=[anywhere] * 9,
        out_specs=pl.BlockSpec(memory_space=pltpu.VMEM),
        scratch_shapes=scratch,
        compiler_params=pltpu.CompilerParams(collective_id=0, has_side_effects=True),
        name="moe_step",
    )(tokens, norm_gain.reshape(1, width), norm_bias.reshape(1, width), group_pick.T, member_pick.T,
      picked_probs.T, gate_weight, up_weight, down_weight)
    return combined.astype(BF16)


def solution(mesh):
    placed = (
        P("ep", "tp"), P("tp"), P("tp"), P("ep", None), P("ep", None), P("ep", None),
        P("ep", "tp", None), P("ep", "tp", None), P("ep", None, "tp"),
    )
    body = functools.partial(per_device, mesh.shape["ep"], mesh.shape["tp"])
    return jax.shard_map(body, mesh=mesh, in_specs=placed, out_specs=P("ep", "tp"), check_vma=False)
```

time: 115 us -> 52.8 us (0.46)
  Pallas kernels: 113 us -> 51.4 us
    pallas_call x1, Pallas kernels: 113 us -> 51.4 us  [per_device(): pl.pallas_call(functools.partial(kernel, E, T, G, cap), out_shape=jax.Sha...]
where the time goes in v1:
time: 52.8 us; the launch traced here: 52.7 us
  Pallas kernels  51.4 us (97%)
  other arithmetic  1.26 us (2%)
    pallas_call x1, Pallas kernels, per_device(): pl.pallas_call(functools.partial(kernel, E, T, G, cap), out_shape=jax.Sha...  51.4 us
    convert_element_type x1, other arithmetic, per_device(): return combined.astype(BF16)  1.26 us

profile of v1, /device:TPU:1, one launch (start us, length us, event | category | flops | bytes accessed | tf_op | source)
XLA Modules:
  0.0 52.7 jit_solution(757280347797197977)
XLA Ops:
  0.0 51.4 %moe_step.1 = f32[8,128]{1,0:T(8,128)} custom-call(bf16[8,128]{1,0:T(8,128)(2,1)} %tokens_h.1, f32[1,128]{1,0:T(1,128)} %bitcast.7, f32[1,128]{1,0:T(1,128)} %bitcast.8, s32[1,8]{1,0:T(1,128)} %bitcast.9, s32[4,8]{1,0:T(4,128)} %bitcast.5, f32[4,8]{1,0:T(4,128)} %bitcast.6, bf16[2,128,1024]{2,1,0:T(8,128)(2,1)} %gate_h.1, bf16[2,128,1024]{2,1,0:T(8,128)(2,1)} %up_h.1, ...), custom_call_target="tpu_custom_call" | custom-call | tf_op jit(solution)/shard_map/moe_step/pallas_call | solution.py:349
  51.4 1.3 %convert_element_type.3 = bf16[8,128]{1,0:T(8,128)(2,1)} convert(f32[8,128]{1,0:T(8,128)} %moe_step.1) | non-fusion elementwise | flops 1024 | bytes 6144 | tf_op jit(solution)/shard_map/convert_element_type | solution.py:359

commit v2 on v1

v2 whole, which is shorter than its diff:
```python
import functools

import jax
import jax.numpy as jnp
from jax import lax
from jax.experimental import pallas as pl
from jax.experimental.pallas import tpu as pltpu
from jax.sharding import PartitionSpec as P

EPG = 8
CORES = 2
LANES = 128
ROW_CHIPS = 4
norm_epsilon = 1e-05
MESH = pl.DeviceIdType.MESH
F32 = jnp.float32
BF16 = jnp.bfloat16


def iota(shape, dim):
    return lax.broadcasted_iota(jnp.int32, shape, dim)


def around(d, size):
    return min(d, size - d)


def kernel(
    E, T, G, cap,
    tokens_h, gain_h, bias_h, group_h, member_h, probs_h, gate_h, up_h, down_h,
    out_ref,
    tokens_v, norm_v, norm_in, group_v, member_v, probs_v, wide_v, down_v,
    stats_out, stats_in, packed_v, rows_v, info_out, info_in, info_all,
    sums_out, sums_in, spread_v, y_out, y_in, hid, expert_v, back_v,
    local_sem, weight_sem, own_sem, swap_s, swap_r,
    stats_s, stats_r, rows_s, rows_r, info_s, info_r, sums_s, sums_r,
    y_s, y_r, hid_s, hid_r, back_s, back_r,
):
    n, width = tokens_h.shape
    NY = T // CORES
    R = E * cap
    group_devices = EPG // CORES
    X = ROW_CHIPS
    Z = E // X
    me = lax.axis_index("ep")
    mt = lax.axis_index("tp")
    core = lax.rem(mt, CORES)
    my = lax.div(mt, CORES)
    mz = lax.div(me, X)
    mx = lax.rem(me, X)
    partner = my * CORES + (1 - core)

    def peer(d):
        dz, dx = divmod(d, X)
        return lax.rem(mz + dz, Z) * X + lax.rem(mx + dx, X)

    def source(d):
        dz, dx = divmod(d, X)
        return lax.rem(mz + Z - dz, Z) * X + lax.rem(mx + X - dx, X)

    def remote(src, dst, ssem, rsem, ep, tp):
        return pltpu.make_async_remote_copy(
            src_ref=src, dst_ref=dst, send_sem=ssem, recv_sem=rsem,
            device_id=(ep, tp), device_id_type=MESH,
        )

    def y_at(o):
        return lax.rem(my + o, NY)

    ep_order = sorted(range(1, E), key=lambda d: -(around(d // X, Z) + around(d % X, X)))
    y_order = sorted(range(1, NY), key=lambda o: -around(o, NY))
    tp_order = sorted(range(1, T), key=lambda t: -around(t // CORES, NY))
    cores = (mt, partner)
    eps = {d: peer(d) for d in ep_order}
    tps = {t: y_at(t // CORES) * CORES + lax.rem(core + t % CORES, CORES) for t in tp_order}

    barrier = pltpu.get_barrier_semaphore()
    for d in ep_order:
        for tp in cores:
            pl.semaphore_signal(barrier, inc=1, device_id=(eps[d], tp), device_id_type=MESH)
    for t in tp_order:
        pl.semaphore_signal(barrier, inc=1, device_id=(me, tps[t]), device_id_type=MESH)

    small = [
        pltpu.make_async_copy(h, v, local_sem.at[i])
        for i, (h, v) in enumerate(
            ((tokens_h, tokens_v), (gain_h, norm_v.at[0]), (bias_h, norm_v.at[1]), (group_h, group_v),
             (member_h, member_v), (probs_h, probs_v))
        )
    ]
    for c in small:
        c.start()
    near = pl.ds(0, width)
    far = pl.ds(width, width)
    weights = [
        pltpu.make_async_copy(gate_h.at[core], wide_v.at[0, near, :], weight_sem.at[0]),
        pltpu.make_async_copy(up_h.at[core], wide_v.at[1, near, :], weight_sem.at[1]),
        pltpu.make_async_copy(down_h.at[core], down_v.at[:, near], weight_sem.at[2]),
    ]
    for c in weights:
        c.start()
    for c in small:
        c.wait()

    lane = iota((n, n), 1)
    sub = iota((n, n), 0)
    spot = iota((n, LANES), 1)

    values = tokens_v[...].astype(F32)
    center_here = jnp.sum(values, axis=1, keepdims=True) / width
    away = values - center_here
    square_here = jnp.sum(away * away, axis=1, keepdims=True)
    stats = jnp.where(spot < LANES // 2, center_here, square_here)
    stats_out[...] = stats
    shifted = (away * norm_v[0]).astype(BF16).astype(F32)

    def column(row):
        wide = jnp.broadcast_to(row, (n, n))
        return jnp.sum(jnp.where(lane == sub, wide, 0.0), axis=1, keepdims=True)

    group_row = group_v[...].astype(F32)
    group_col = column(group_row)
    same = jnp.where(group_col == group_row, 1.0, 0.0)
    slot_row = jnp.sum(jnp.where(sub < lane, same, 0.0), axis=0, keepdims=True)
    slot_col = jnp.sum(jnp.where(lane < sub, same, 0.0), axis=1, keepdims=True)
    place = jnp.where(iota((G * cap, n), 0).astype(F32) == group_row * cap + slot_row, 1.0, 0.0)
    packed = place[:, 0:1] * shifted[0:1, :]
    for t in range(1, n):
        packed += place[:, t : t + 1] * shifted[t : t + 1, :]
    packed_v[...] = packed

    pl.semaphore_wait(barrier, CORES * (E - 1) + T - 1)

    def group_rows(ep):
        return packed_v.at[pl.ds(lax.div(ep, group_devices) * cap, cap), :]

    def slot_rows(d, rel):
        return rows_v.at[pl.ds(d * cap, cap), pl.ds(rel * width, width)]

    sent = []
    for d in ep_order:
        for rel, tp in enumerate(cores):
            c = remote(
                group_rows(eps[d]), slot_rows(d, rel), rows_s.at[rel, d], rows_r.at[rel, d], eps[d], tp,
            )
            c.start()
            sent.append(c)
    c = remote(group_rows(me), slot_rows(0, 1), rows_s.at[1, 0], rows_r.at[1, 0], me, partner)
    c.start()
    sent.append(c)
    own_rows = pltpu.make_async_copy(group_rows(me), slot_rows(0, 0), own_sem.at[0])
    own_rows.start()
    told = []
    for t in tp_order:
        c = remote(stats_out, stats_in.at[t], stats_s.at[t], stats_r.at[t], me, tps[t])
        c.start()
        told.append(c)
    swaps = [
        remote(norm_v, norm_in, swap_s.at[0], swap_r.at[0], me, partner),
        remote(gate_h.at[1 - core], wide_v.at[0, far, :], swap_s.at[1], swap_r.at[1], me, partner),
        remote(up_h.at[1 - core], wide_v.at[1, far, :], swap_s.at[2], swap_r.at[2], me, partner),
        remote(down_h.at[1 - core], down_v.at[:, far], swap_s.at[3], swap_r.at[3], me, partner),
    ]
    for c in swaps:
        c.start()

    probs = probs_v[...]
    member = member_v[...].astype(F32)
    shares = probs / jnp.sum(probs, axis=0, keepdims=True)
    back_lane = iota((n, 2 * R), 1)
    back_slot = lax.rem(back_lane, cap).astype(F32)
    back_ep = lax.div(lax.rem(back_lane, R), cap)
    back_group = lax.div(back_ep, group_devices).astype(F32)
    back_core = jnp.where(back_lane < R, core, 1 - core)
    back_member = (lax.rem(back_ep, group_devices) * CORES + back_core).astype(F32)
    mixing = jnp.zeros((n, 2 * R), F32)
    for k in range(probs.shape[0]):
        mixing += jnp.where(back_member == column(member[k : k + 1, :]), column(shares[k : k + 1, :]), 0.0)
    here = jnp.where(back_group == group_col, 1.0, 0.0) * jnp.where(back_slot == slot_col, 1.0, 0.0)
    mixing = mixing * here
    mixing_high = mixing.astype(BF16).astype(F32)
    mixing = jnp.concatenate([mixing_high, mixing - mixing_high], axis=0).astype(BF16)

    spread_v[...] = jnp.zeros(spread_v.shape, F32)
    for c in weights[:2]:
        c.wait()
    for c in swaps[:3]:
        c.wait_recv()
    gains = (norm_v[0], norm_in[0])
    biases = (norm_v[1], norm_in[1])
    row16 = iota((16, width), 0)

    def factors(w, rel):
        total = jnp.zeros((16, width), F32)
        for at, v in ((2 * rel, gains[rel]), (4, biases[rel])):
            high = v.astype(BF16).astype(F32)
            total += jnp.where(row16 == at + w, high, 0.0) + jnp.where(row16 == at + w + 8, v - high, 0.0)
        return total

    sums = jnp.zeros((16, wide_v.shape[2]), F32)
    for w in range(2):
        both = jnp.concatenate([factors(w, 0), factors(w, 1)], axis=1).astype(BF16)
        sums += jnp.dot(both, wide_v[w], preferred_element_type=F32)
    sums = sums[0:8, :] + sums[8:16, :]
    for y in range(NY):
        sums_out[y] = sums[:, y * LANES : (y + 1) * LANES]
    to_sums = {}
    for o in y_order:
        c = remote(
            sums_out.at[y_at(o)], sums_in.at[o], sums_s.at[o], sums_r.at[o], me, y_at(o) * CORES + core,
        )
        c.start()
        to_sums[o] = c
    sums_in[0] = sums_out[my]

    own_rows.wait()
    for c in sent:
        c.wait_recv()
    rows = rows_v[...].astype(BF16)

    def product(w, y):
        block = wide_v[w, :, pl.ds(pl.multiple_of(y * LANES, LANES), LANES)]
        return jnp.dot(rows, block, preferred_element_type=F32)

    to_y = {}
    for o in y_order:
        for w in range(2):
            y_out[o, w] = product(w, y_at(o)).astype(BF16)
        c = remote(
            y_out.at[o], y_in.at[o], y_s.at[o], y_r.at[o], me, y_at(o) * CORES + core,
        )
        c.start()
        to_y[o] = c

    for c in told:
        c.wait_recv()
    heard = [stats] + [stats_in[t] for t in range(1, T)]
    total = heard[0]
    for h in heard[1:]:
        total += h
    center = total / T
    moved = jnp.zeros((n, LANES), F32)
    for h in heard:
        moved += (h - center) * (h - center)
    inner = jnp.where(spot == 0, width * moved, 0.0) + jnp.where(spot == LANES // 2, total, 0.0)
    spread = jnp.sum(inner, axis=1, keepdims=True) / (width * T)
    factor = lax.rsqrt(spread + norm_epsilon)
    spot_f = spot.astype(F32)
    info = jnp.where(spot_f == slot_col, factor, 0.0)
    for k in range(T):
        info += jnp.where(spot_f == slot_col + (k + 1) * cap, (heard[k] - center) * factor, 0.0)
    for g in range(G):
        info_out[g] = jnp.sum(jnp.where(group_col == g, info, 0.0), axis=0, keepdims=True)
    to_info = {}
    for d in ep_order:
        c = remote(
            info_out.at[lax.div(eps[d], group_devices)], info_in.at[d], info_s.at[d], info_r.at[d], eps[d], mt,
        )
        c.start()
        to_info[d] = c
    info_in[0] = info_out[lax.div(me, group_devices)]

    gate = product(0, my)
    up = product(1, my)

    for o in y_order:
        to_sums[o].wait_recv()
    base_gate = jnp.zeros((1, LANES), F32)
    base_up = jnp.zeros((1, LANES), F32)
    for o in range(NY):
        block = sums_in[o]
        for rel in range(CORES):
            at = (2 * o + rel + 1) * cap
            for w in range(2):
                line = block[2 * rel + w : 2 * rel + w + 1, :]
                spread_v[w, at : at + cap, :] = jnp.broadcast_to(line, (cap, LANES))
        base_gate += block[4:5, :]
        base_up += block[5:6, :]
    for d in ep_order:
        to_info[d].wait_recv()
    for d in range(E):
        info_all[d * cap : (d + 1) * cap, :] = jnp.broadcast_to(info_in[d], (cap, LANES))
    rlane = iota((R, LANES), 1)
    rslot = lax.rem(iota((R, LANES), 0), cap)
    facts = jnp.where(lax.rem(rlane, cap) == rslot, info_all[...], 0.0)
    scale = jnp.sum(jnp.where(rlane < cap, facts, 0.0), axis=1, keepdims=True)

    def extra(w):
        return jnp.dot(facts, spread_v[w], preferred_element_type=F32, precision=lax.Precision.HIGHEST)

    extra_gate = extra(0) + base_gate
    extra_up = extra(1) + base_up

    for o in reversed(y_order):
        to_y[o].wait_recv()
        gate += y_in[o, 0].astype(F32)
        up += y_in[o, 1].astype(F32)
    gate = gate * scale + extra_gate
    up = up * scale + extra_up
    hid[my] = (gate / (1.0 + jnp.exp(-gate)) * up).astype(BF16)
    to_hid = {}
    for o in y_order:
        c = remote(
            hid.at[my], hid.at[my], hid_s.at[o], hid_r.at[o], me, y_at(o) * CORES + core,
        )
        c.start()
        to_hid[o] = c
    weights[2].wait()
    swaps[3].wait_recv()

    def down(o):
        at = lax.rem(my + NY - o, NY)
        block = down_v[pl.ds(pl.multiple_of(at * LANES, LANES), LANES), :]
        return jnp.dot(hid[at], block, preferred_element_type=F32)

    expert = down(0)
    for o in reversed(y_order):
        to_hid[o].wait_recv()
        expert += down(o)
    expert_v[...] = expert.astype(BF16).astype(F32)

    def expert_rows(d, rel):
        return expert_v.at[pl.ds(d * cap, cap), pl.ds(rel * width, width)]

    def back_rows(rel):
        return back_v.at[pl.ds(rel * R + me * cap, cap), :]

    back = []
    for d in ep_order:
        to = source(d)
        for rel, tp in enumerate(cores):
            c = remote(expert_rows(d, rel), back_rows(rel), back_s.at[rel, d], back_r.at[rel, d], to, tp)
            c.start()
            back.append(c)
    c = remote(expert_rows(0, 1), back_rows(1), back_s.at[1, 0], back_r.at[1, 0], me, partner)
    c.start()
    back.append(c)
    own_back = pltpu.make_async_copy(expert_rows(0, 0), back_rows(0), own_sem.at[1])
    own_back.start()
    for c in sent + told + swaps:
        c.wait_send()
    for held in (to_sums, to_y, to_info, to_hid):
        for c in held.values():
            c.wait_send()
    own_back.wait()
    for c in back:
        c.wait_recv()
    mixed = jnp.dot(mixing, back_v[...].astype(BF16), preferred_element_type=F32)
    out_ref[...] = mixed[0:n, :] + mixed[n : 2 * n, :]
    for c in back:
        c.wait_send()


def per_device(E, T, tokens, norm_gain, norm_bias, group_pick, member_pick, picked_probs,
               gate_weight, up_weight, down_weight):
    n, width = tokens.shape
    LE, _, FF = gate_weight.shape
    NY = T // CORES
    G = LE * E // EPG
    cap = max(n // 4, (n + G - 1) // G)
    R = E * cap
    k = picked_probs.shape[1]
    dma = pltpu.SemaphoreType.DMA
    V = pltpu.VMEM
    scratch = [
        V((n, width), BF16), V((2, 1, width), F32), V((2, 1, width), F32),
        V((1, n), jnp.int32), V((k, n), jnp.int32), V((k, n), F32),
        V((2, 2 * width, FF), BF16), V((FF, 2 * width), BF16),
        V((n, LANES), F32), V((T, n, LANES), F32), V((G * cap, width), F32), V((R, 2 * width), F32),
        V((G, 1, LANES), F32), V((E, 1, LANES), F32), V((R, LANES), F32),
        V((NY, 8, LANES), F32), V((NY, 8, LANES), F32), V((2, LANES, LANES), F32),
        V((NY, 2, R, LANES), BF16), V((NY, 2, R, LANES), BF16),
        V((NY, R, LANES), BF16), V((R, 2 * width), F32), V((2 * R, width), F32),
        dma((6,)), dma((3,)), dma((2,)), dma((4,)), dma((4,)),
        dma((T,)), dma((T,)), dma((2, E)), dma((2, E)), dma((E,)), dma((E,)), dma((NY,)), dma((NY,)),
        dma((NY,)), dma((NY,)), dma((NY,)), dma((NY,)), dma((2, E)), dma((2, E)),
    ]
    anywhere = pl.BlockSpec(memory_space=pl.ANY)
    combined = pl.pallas_call(
        functools.partial(kernel, E, T, G, cap),
        out_shape=jax.ShapeDtypeStruct((n, width), F32),
        in_specs=[anywhere] * 9,
        out_specs=pl.BlockSpec(memory_space=pltpu.VMEM),
        scratch_shapes=scratch,
        compiler_params=pltpu.CompilerParams(collective_id=0, has_side_effects=True),
        name="moe_step",
    )(tokens, norm_gain.reshape(1, width), norm_bias.reshape(1, width), group_pick.T, member_pick.T,
      picked_probs.T, gate_weight, up_weight, down_weight)
    return combined.astype(BF16)


def solution(mesh):
    placed = (
        P("ep", "tp"), P("tp"), P("tp"), P("ep", None), P("ep", None), P("ep", None),
        P("ep", "tp", None), P("ep", "tp", None), P("ep", None, "tp"),
    )
    body = functools.partial(per_device, mesh.shape["ep"], mesh.shape["tp"])
    return jax.shard_map(body, mesh=mesh, in_specs=placed, out_specs=P("ep", "tp"), check_vma=False)
```

time: 52.8 us -> 49.2 us (0.932)
  Pallas kernels: 51.4 us -> 47.8 us
    pallas_call x1, Pallas kernels: 51.4 us -> 47.8 us  [per_device(): pl.pallas_call(functools.partial(kernel, E, T, G, cap), out_shape=jax.Sha...]
where the time goes in v2:
time: 49.2 us; the launch traced here: 49 us
  Pallas kernels  47.8 us (97%)
  other arithmetic  1.26 us (3%)
    pallas_call x1, Pallas kernels, per_device(): pl.pallas_call(functools.partial(kernel, E, T, G, cap), out_shape=jax.Sha...  47.8 us
    convert_element_type x1, other arithmetic, per_device(): return combined.astype(BF16)  1.26 us

profile of v2, /device:TPU:1, one launch (start us, length us, event | category | flops | bytes accessed | tf_op | source)
XLA Modules:
  0.0 49.0 jit_solution(17025055428235096163)
XLA Ops:
  0.0 47.8 %moe_step.1 = f32[8,128]{1,0:T(8,128)} custom-call(bf16[8,128]{1,0:T(8,128)(2,1)} %tokens_h.1, f32[1,128]{1,0:T(1,128)} %bitcast.7, f32[1,128]{1,0:T(1,128)} %bitcast.8, s32[1,8]{1,0:T(1,128)} %bitcast.9, s32[4,8]{1,0:T(4,128)} %bitcast.5, f32[4,8]{1,0:T(4,128)} %bitcast.6, bf16[2,128,1024]{2,1,0:T(8,128)(2,1)} %gate_h.1, bf16[2,128,1024]{2,1,0:T(8,128)(2,1)} %up_h.1, ...), custom_call_target="tpu_custom_call" | custom-call | tf_op jit(solution)/shard_map/moe_step/pallas_call | solution.py:379
  47.8 1.3 %convert_element_type.3 = bf16[8,128]{1,0:T(8,128)(2,1)} convert(f32[8,128]{1,0:T(8,128)} %moe_step.1) | non-fusion elementwise | flops 1024 | bytes 6144 | tf_op jit(solution)/shard_map/convert_element_type | solution.py:389

commit v3 on v2

--- a/solution.py
+++ b/solution.py
@@ -32,7 +32,7 @@
     tokens_v, norm_v, norm_in, group_v, member_v, probs_v, wide_v, down_v,
     stats_out, stats_in, packed_v, rows_v, info_out, info_in, info_all,
     sums_out, sums_in, spread_v, y_out, y_in, hid, expert_v, back_v,
-    local_sem, weight_sem, own_sem, swap_s, swap_r,
+    local_sem, weight_sem, swap_s, swap_r,
     stats_s, stats_r, rows_s, rows_r, info_s, info_r, sums_s, sums_r,
     y_s, y_r, hid_s, hid_r, back_s, back_r,
 ):
@@ -67,6 +67,9 @@
     def y_at(o):
         return lax.rem(my + o, NY)
 
+    def await_all(ref, sem):
+        pltpu.make_async_copy(ref, ref, sem).wait()
+
     ep_order = sorted(range(1, E), key=lambda d: -(around(d // X, Z) + around(d % X, X)))
     y_order = sorted(range(1, NY), key=lambda o: -around(o, NY))
     tp_order = sorted(range(1, T), key=lambda t: -around(t // CORES, NY))
@@ -137,24 +140,19 @@
     def slot_rows(d, rel):
         return rows_v.at[pl.ds(d * cap, cap), pl.ds(rel * width, width)]
 
-    sent = []
     for d in ep_order:
         for rel, tp in enumerate(cores):
             c = remote(
-                group_rows(eps[d]), slot_rows(d, rel), rows_s.at[rel, d], rows_r.at[rel, d], eps[d], tp,
+                group_rows(eps[d]), slot_rows(d, rel), rows_s, rows_r, eps[d], tp,
             )
             c.start()
-            sent.append(c)
-    c = remote(group_rows(me), slot_rows(0, 1), rows_s.at[1, 0], rows_r.at[1, 0], me, partner)
+    c = remote(group_rows(me), slot_rows(0, 1), rows_s, rows_r, me, partner)
     c.start()
-    sent.append(c)
-    own_rows = pltpu.make_async_copy(group_rows(me), slot_rows(0, 0), own_sem.at[0])
+    own_rows = pltpu.make_async_copy(group_rows(me), slot_rows(0, 0), rows_r)
     own_rows.start()
-    told = []
     for t in tp_order:
-        c = remote(stats_out, stats_in.at[t], stats_s.at[t], stats_r.at[t], me, tps[t])
-        c.start()
-        told.append(c)
+        c = remote(stats_out, stats_in.at[t], stats_s, stats_r, me, tps[t])
+        c.start()
     swaps = [
         remote(norm_v, norm_in, swap_s.at[0], swap_r.at[0], me, partner),
         remote(gate_h.at[1 - core], wide_v.at[0, far, :], swap_s.at[1], swap_r.at[1], me, partner),
@@ -204,36 +202,29 @@
     sums = sums[0:8, :] + sums[8:16, :]
     for y in range(NY):
         sums_out[y] = sums[:, y * LANES : (y + 1) * LANES]
-    to_sums = {}
     for o in y_order:
         c = remote(
-            sums_out.at[y_at(o)], sums_in.at[o], sums_s.at[o], sums_r.at[o], me, y_at(o) * CORES + core,
-        )
-        c.start()
-        to_sums[o] = c
+            sums_out.at[y_at(o)], sums_in.at[o], sums_s, sums_r, me, y_at(o) * CORES + core,
+        )
+        c.start()
     sums_in[0] = sums_out[my]
 
-    own_rows.wait()
-    for c in sent:
-        c.wait_recv()
+    await_all(rows_v, rows_r)
     rows = rows_v[...].astype(BF16)
 
     def product(w, y):
         block = wide_v[w, :, pl.ds(pl.multiple_of(y * LANES, LANES), LANES)]
         return jnp.dot(rows, block, preferred_element_type=F32)
 
-    to_y = {}
     for o in y_order:
         for w in range(2):
             y_out[o, w] = product(w, y_at(o)).astype(BF16)
         c = remote(
-            y_out.at[o], y_in.at[o], y_s.at[o], y_r.at[o], me, y_at(o) * CORES + core,
-        )
-        c.start()
-        to_y[o] = c
-
-    for c in told:
-        c.wait_recv()
+            y_out.at[o], y_in.at[o], y_s, y_r, me, y_at(o) * CORES + core,
+        )
+        c.start()
+
+    await_all(stats_in.at[pl.ds(1, T - 1)], stats_r)
     heard = [stats] + [stats_in[t] for t in range(1, T)]
     total = heard[0]
     for h in heard[1:]:
@@ -251,20 +242,17 @@
         info += jnp.where(spot_f == slot_col + (k + 1) * cap, (heard[k] - center) * factor, 0.0)
     for g in range(G):
         info_out[g] = jnp.sum(jnp.where(group_col == g, info, 0.0), axis=0, keepdims=True)
-    to_info = {}
     for d in ep_order:
         c = remote(
-            info_out.at[lax.div(eps[d], group_devices)], info_in.at[d], info_s.at[d], info_r.at[d], eps[d], mt,
-        )
-        c.start()
-        to_info[d] = c
+            info_out.at[lax.div(eps[d], group_devices)], info_in.at[d], info_s, info_r, eps[d], mt,
+        )
+        c.start()
     info_in[0] = info_out[lax.div(me, group_devices)]
 
     gate = product(0, my)
     up = product(1, my)
 
-    for o in y_order:
-        to_sums[o].wait_recv()
+    await_all(sums_in.at[pl.ds(1, NY - 1)], sums_r)
     base_gate = jnp.zeros((1, LANES), F32)
     base_up = jnp.zeros((1, LANES), F32)
     for o in range(NY):
@@ -276,8 +264,7 @@
                 spread_v[w, at : at + cap, :] = jnp.broadcast_to(line, (cap, LANES))
         base_gate += block[4:5, :]
         base_up += block[5:6, :]
-    for d in ep_order:
-        to_info[d].wait_recv()
+    await_all(info_in.at[pl.ds(1, E - 1)], info_r)
     for d in range(E):
         info_all[d * cap : (d + 1) * cap, :] = jnp.broadcast_to(info_in[d], (cap, LANES))
     rlane = iota((R, LANES), 1)
@@ -291,8 +278,8 @@
     extra_gate = extra(0) + base_gate
     extra_up = extra(1) + base_up
 
-    for o in reversed(y_order):
-        to_y[o].wait_recv()
+    await_all(y_in.at[pl.ds(1, NY - 1)], y_r)
+    for o in range(1, NY):
         gate += y_in[o, 0].astype(F32)
         up += y_in[o, 1].astype(F32)
     gate = gate * scale + extra_gate
@@ -301,7 +288,7 @@
     to_hid = {}
     for o in y_order:
         c = remote(
-            hid.at[my], hid.at[my], hid_s.at[o], hid_r.at[o], me, y_at(o) * CORES + core,
+            hid.at[my], hid.at[my], hid_s, hid_r.at[o], me, y_at(o) * CORES + core,
         )
         c.start()
         to_hid[o] = c
@@ -325,30 +312,27 @@
     def back_rows(rel):
         return back_v.at[pl.ds(rel * R + me * cap, cap), :]
 
-    back = []
     for d in ep_order:
         to = source(d)
         for rel, tp in enumerate(cores):
-            c = remote(expert_rows(d, rel), back_rows(rel), back_s.at[rel, d], back_r.at[rel, d], to, tp)
+            c = remote(expert_rows(d, rel), back_rows(rel), back_s, back_r, to, tp)
             c.start()
-            back.append(c)
-    c = remote(expert_rows(0, 1), back_rows(1), back_s.at[1, 0], back_r.at[1, 0], me, partner)
+    c = remote(expert_rows(0, 1), back_rows(1), back_s, back_r, me, partner)
     c.start()
-    back.append(c)
-    own_back = pltpu.make_async_copy(expert_rows(0, 0), back_rows(0), own_sem.at[1])
+    own_back = pltpu.make_async_copy(expert_rows(0, 0), back_rows(0), back_r)
     own_back.start()
-    for c in sent + told + swaps:
+    for c in swaps:
         c.wait_send()
-    for held in (to_sums, to_y, to_info, to_hid):
-        for c in held.values():
-            c.wait_send()
-    own_back.wait()
-    for c in back:
-        c.wait_recv()
+    await_all(back_v.at[pl.ds(0, 2 * R - cap), :], rows_s)
+    await_all(stats_in.at[pl.ds(1, T - 1)], stats_s)
+    await_all(sums_in.at[pl.ds(1, NY - 1)], sums_s)
+    await_all(info_in.at[pl.ds(1, E - 1)], info_s)
+    await_all(y_in.at[pl.ds(1, NY - 1)], y_s)
+    await_all(hid.at[pl.ds(1, NY - 1)], hid_s)
+    await_all(back_v, back_r)
     mixed = jnp.dot(mixing, back_v[...].astype(BF16), preferred_element_type=F32)
     out_ref[...] = mixed[0:n, :] + mixed[n : 2 * n, :]
-    for c in back:
-        c.wait_send()
+    await_all(back_v.at[pl.ds(0, 2 * R - cap), :], back_s)
 
 
 def per_device(E, T, tokens, norm_gain, norm_bias, group_pick, member_pick, picked_probs,
@@ -371,9 +355,9 @@
         V((NY, 8, LANES), F32), V((NY, 8, LANES), F32), V((2, LANES, LANES), F32),
         V((NY, 2, R, LANES), BF16), V((NY, 2, R, LANES), BF16),
         V((NY, R, LANES), BF16), V((R, 2 * width), F32), V((2 * R, width), F32),
-        dma((6,)), dma((3,)), dma((2,)), dma((4,)), dma((4,)),
-        dma((T,)), dma((T,)), dma((2, E)), dma((2, E)), dma((E,)), dma((E,)), dma((NY,)), dma((NY,)),
-        dma((NY,)), dma((NY,)), dma((NY,)), dma((NY,)), dma((2, E)), dma((2, E)),
+        dma((6,)), dma((3,)), dma((4,)), dma((4,)),
+        dma, dma, dma, dma, dma, dma, dma, dma,
+        dma, dma, dma, dma((NY,)), dma, dma,
     ]
     anywhere = pl.BlockSpec(memory_space=pl.ANY)
     combined = pl.pallas_call(

time: 49.2 us -> 45.9 us (0.933)
  Pallas kernels: 47.8 us -> 44.5 us
    pallas_call x1, Pallas kernels: 47.8 us -> 44.5 us  [per_device(): pl.pallas_call(functools.partial(kernel, E, T, G, cap), out_shape=jax.Sha...]
where the time goes in v3:
time: 45.9 us; the launch traced here: 45.7 us
  Pallas kernels  44.5 us (97%)
  other arithmetic  1.26 us (3%)
    pallas_call x1, Pallas kernels, per_device(): pl.pallas_call(functools.partial(kernel, E, T, G, cap), out_shape=jax.Sha...  44.5 us
    convert_element_type x1, other arithmetic, per_device(): return combined.astype(BF16)  1.26 us

profile of v3, /device:TPU:1, one launch (start us, length us, event | category | flops | bytes accessed | tf_op | source)
XLA Modules:
  0.0 45.7 jit_solution(4979313472774230005)
XLA Ops:
  0.0 44.5 %moe_step.1 = f32[8,128]{1,0:T(8,128)} custom-call(bf16[8,128]{1,0:T(8,128)(2,1)} %tokens_h.1, f32[1,128]{1,0:T(1,128)} %bitcast.7, f32[1,128]{1,0:T(1,128)} %bitcast.8, s32[1,8]{1,0:T(1,128)} %bitcast.9, s32[4,8]{1,0:T(4,128)} %bitcast.5, f32[4,8]{1,0:T(4,128)} %bitcast.6, bf16[2,128,1024]{2,1,0:T(8,128)(2,1)} %gate_h.1, bf16[2,128,1024]{2,1,0:T(8,128)(2,1)} %up_h.1, ...), custom_call_target="tpu_custom_call" | custom-call | tf_op jit(solution)/shard_map/moe_step/pallas_call | solution.py:363
  44.5 1.3 %convert_element_type.3 = bf16[8,128]{1,0:T(8,128)(2,1)} convert(f32[8,128]{1,0:T(8,128)} %moe_step.1) | non-fusion elementwise | flops 1024 | bytes 6144 | tf_op jit(solution)/shard_map/convert_element_type | solution.py:373
